TPU v7x, 32 devices: a whole 2x2x4 slice. The times are simulated.
32 devices in a mesh: rep: 4 (over z), fs: 4 (over y, x), tp: 2 (over core).
Axes of the slice: x: 2, y: 2, z: 4, core: 2. Of those that a mesh axis runs over, the one named last changes fastest.
Arguments:
- skip_stream_entry: bfloat16 [4096, 2048], P(('rep', 'fs')), may hold values from -6 to 6
- sequence_blender_factor: float32 [2048], replicated, may hold values from 0.1 to 1.9
- product_projector: float32 [2048, 1024], P('fs', 'tp'), may hold values from -0.125 to 0.125
- product_side_factors: float32 [1024], P('tp'), may hold values from 0.3 to 3
- placewise_projector: float32 [2048, 1024], P('fs', 'tp'), may hold values from -0.125 to 0.125
- placewise_entry_factors: float32 [1024], P('tp'), may hold values from 0.7 to 11.2, as said below
- placewise_rescale_factor: float32 [1024], P('tp'), may hold values from 0.1 to 1.9
- place_cluster_operator: bfloat16 [8, 128, 128], replicated, may hold values from -0.5 to 0.5
- placewise_offset_vector: float32 [8, 128], replicated, may hold values from 0.1 to 1.9
- blender_result_projector: float32 [1024, 2048], P('tp', 'fs'), may hold values from -0.1875 to 0.1875
- blender_result_factors: float32 [2048], P('fs'), may hold values from 0.3 to 3
- feedforward_norm_factor: float32 [2048], replicated, may hold values from 0.1 to 1.9
- switch_projector: float32 [2048, 2816], P('fs', 'tp'), may hold values from -0.125 to 0.125
- switch_factors: float32 [2816], P('tp'), may hold values from 0.3 to 3
- expand_projector: float32 [2048, 2816], P('fs', 'tp'), may hold values from -0.125 to 0.125
- expand_factors: float32 [2816], P('tp'), may hold values from 0.3 to 3
- contract_projector: float32 [2816, 2048], P('tp', 'fs'), may hold values from -0.109375 to 0.109375
- contract_factors: float32 [2048], P('fs'), may hold values from 0.3 to 3
Outputs:
- result: bfloat16 [4096, 2048], P(('rep', 'fs'), 'tp')
Inputs may be any that keep to these rules, and one draw needn't show every extreme that they name: `placewise_entry_factors`: positive column scales.
All inputs are finite; a program needn't handle non-finite values.
Results may differ from a plain program's by a relative error of at most 0.023.
Values may be sent and summed in bfloat16 or wider, within the bound.
A program may use at most 64 MiB of HBM per device.

v0:
```python
import jax
import jax.numpy as jnp
from jax import lax
from jax.sharding import PartitionSpec as P

BLENDER_FEATURES = 1024
GROUP_DIM = 128
BLOCK = 128


epsilon = 1e-06


def normalize(values, gain):
    return values * lax.rsqrt(jnp.mean(values * values, axis=-1, keepdims=True) + epsilon) * gain


def assembled_entries(pieces, activations):
    segments = (
        lax.all_gather(pieces[0], "fs", axis=0, tiled=True),
        lax.all_gather(pieces[1], "fs", axis=0, tiled=True),
    )
    return tuple(
        (jnp.dot(activations, segment, preferred_element_type=jnp.float32) for segment in segments)
    )


def collect_cols(shard_rows, activations, scales):
    return (
        jnp.dot(
            activations,
            lax.all_gather(shard_rows, "fs", axis=1, tiled=True),
            preferred_element_type=jnp.float32,
        )
        * scales
    )


def on_device(
    skip_stream_entry,
    sequence_blender_factor,
    product_projector,
    product_side_factors,
    placewise_projector,
    placewise_entry_factors,
    placewise_rescale_factor,
    place_cluster_operator,
    placewise_offset_vector,
    blender_result_projector,
    blender_result_factors,
    feedforward_norm_factor,
    switch_projector,
    switch_factors,
    expand_projector,
    expand_factors,
    contract_projector,
    contract_factors,
):
    device_sequence_steps = skip_stream_entry.shape[0]
    tp_index = lax.axis_index("tp")
    own_features = skip_stream_entry.shape[1] // lax.axis_size("tp")
    out_scales = (
        lax.all_gather(blender_result_factors, "fs", axis=0, tiled=True),
        lax.all_gather(contract_factors, "fs", axis=0, tiled=True),
    )
    standardized_stream = normalize(
        skip_stream_entry.astype(jnp.float32), sequence_blender_factor
    ).astype(jnp.bfloat16)
    product_plain, diffuse_plain = assembled_entries(
        (product_projector.astype(jnp.bfloat16), placewise_projector.astype(jnp.bfloat16)),
        standardized_stream,
    )
    product_portion = jax.nn.gelu(product_plain * product_side_factors)
    spread = jax.nn.gelu(diffuse_plain * placewise_entry_factors)
    feature_total = spread.shape[1]
    squares = lax.psum(jnp.sum(spread * spread, axis=1), "tp")
    factor = lax.rsqrt(squares / BLENDER_FEATURES + epsilon)
    spread_normed = (spread * factor[:, None] * placewise_rescale_factor).astype(jnp.bfloat16)
    group_span = min(feature_total, GROUP_DIM)
    group_count = max(1, feature_total // GROUP_DIM)
    first_group = tp_index * feature_total // GROUP_DIM
    causal = jnp.tril(jnp.ones((BLOCK, BLOCK), dtype=bool))
    local_weight = lax.dynamic_slice_in_dim(place_cluster_operator, first_group, group_count, 0)
    local_weight = jnp.where(causal[None], local_weight, jnp.zeros_like(local_weight))
    local_bias = lax.dynamic_slice_in_dim(placewise_offset_vector, first_group, group_count, 0)
    blocks = spread_normed.reshape(device_sequence_steps // BLOCK, BLOCK, group_count, group_span)
    blended_sequence = jnp.einsum(
        "gts,nsgc->ntgc", local_weight, blocks, preferred_element_type=jnp.float32
    )
    blended_sequence = blended_sequence + local_bias.T[None, :, :, None]
    switched_inner = (
        product_portion * blended_sequence.reshape(device_sequence_steps, feature_total)
    ).astype(jnp.bfloat16)
    mix_terms = collect_cols(
        blender_result_projector.astype(jnp.bfloat16), switched_inner, out_scales[0]
    )
    mix_total = lax.psum_scatter(
        mix_terms.astype(jnp.bfloat16), "tp", scatter_dimension=1, tiled=True
    ).astype(jnp.float32)
    own_input = lax.dynamic_slice_in_dim(
        skip_stream_entry, tp_index * own_features, own_features, 1
    )
    stream = (own_input.astype(jnp.float32) + mix_total).astype(jnp.bfloat16)
    stream_whole = lax.all_gather(stream, "tp", axis=1, tiled=True)
    ffn_normed = normalize(stream_whole.astype(jnp.float32), feedforward_norm_factor).astype(
        jnp.bfloat16
    )
    gate_raw, up_raw = assembled_entries(
        (switch_projector.astype(jnp.bfloat16), expand_projector.astype(jnp.bfloat16)), ffn_normed
    )
    active = (jax.nn.silu(gate_raw * switch_factors) * (up_raw * expand_factors)).astype(
        jnp.bfloat16
    )
    ffn_terms = collect_cols(contract_projector.astype(jnp.bfloat16), active, out_scales[1])
    ffn_total = lax.psum_scatter(
        ffn_terms.astype(jnp.bfloat16), "tp", scatter_dimension=1, tiled=True
    ).astype(jnp.float32)
    return (stream.astype(jnp.float32) + ffn_total).astype(jnp.bfloat16)


def solution(mesh):
    return jax.shard_map(
        on_device,
        mesh=mesh,
        in_specs=(
            P(("rep", "fs"), None),
            P(),
            P("fs", "tp"),
            P("tp"),
            P("fs", "tp"),
            P("tp"),
            P("tp"),
            P(),
            P(),
            P("tp", "fs"),
            P("fs"),
            P(),
            P("fs", "tp"),
            P("tp"),
            P("fs", "tp"),
            P("tp"),
            P("tp", "fs"),
            P("fs"),
        ),
        out_specs=P(("rep", "fs"), "tp"),
        check_vma=False,
    )
```

profile of v0, /device:TPU:1, one launch (start us, length us, event | category | flops | bytes accessed | tf_op | source)
XLA Modules:
  0.0 376.3 jit_solution(2161271477478694587)
XLA Ops:
  6.5 2.2 convert_element_type.67
  8.8 0.0 all-gather.10.cloned.1.call-start
  8.9 0.9 convert_element_type.66
  9.8 0.0 all-gather.14.cloned.1.call-start
  9.9 0.9 convert_element_type.70
  10.8 0.0 reduce-scatter.3.cloned.1.call-start
  10.8 6.9 %all-gather = f32[4,1,512]{2,1,0:T(1,128)S(1)} all-gather(f32[1,1,512]{2,1,0:T(1,128)S(1)} %bitcast.31), channel_id=1, replica_groups=mesh['rep'=4,'fs'=4,'tp'=2] {'fs'}, dimensions={0}, use_global_device_ids=true | all-gather | bytes 10240 | tf_op jit(solution)/shard_map/all_gather | solution.py:63
  17.8 0.3 fusion.4
  18.1 28.2 %all-gather.12.cloned.1.call-done = bf16[2048,512]{1,0:T(8,128)(2,1)} async-done(((bf16[512,512]{1,0:T(8,128)(2,1)}), bf16[2048,512]{1,0:T(8,128)(2,1)}) %all-gather.12.cloned.1.call-update) | async-done | bytes 2097168 | tf_op jit(solution)/shard_map/all_gather | solution.py:21
  46.3 2.6 multiply_reduce_fusion
  48.9 3.0 psum.7
  51.9 0.1 multiply_convert_fusion
  52.0 0.1 reshape.40
  52.1 0.3 fusion.10
  52.3 0.2 copy.22
  52.6 30.8 %all-gather.10.cloned.1.call-done = bf16[2048,512]{1,0:T(8,128)(2,1)} async-done(((bf16[512,512]{1,0:T(8,128)(2,1)}), bf16[2048,512]{1,0:T(8,128)(2,1)}) %all-gather.10.cloned.1.call-update) | async-done | bytes 2097168 | tf_op jit(solution)/shard_map/all_gather | solution.py:20
  83.3 36.9 %all-gather.14.cloned.1.call-done = bf16[512,2048]{1,0:T(8,128)(2,1)} async-done(((bf16[512,512]{1,0:T(8,128)(2,1)}), bf16[512,2048]{1,0:T(8,128)(2,1)}) %all-gather.14.cloned.1.call-update) | async-done | bytes 2097168 | tf_op jit(solution)/shard_map/all_gather | solution.py:32
  120.3 4.8 %fusion.1 = bf16[256,2048]{1,0:T(8,128)(2,1)} fusion(bf16[512,2048]{1,0:T(8,128)(2,1)} %all-gather.14.cloned.1.call-done, f32[2048]{0:T(1024)S(1)} %bitcast.29, bf16[2048,512]{1,0:T(8,128)(2,1)} %all-gather.10.cloned.1.call-done, f32[32,8,4,128]{3,2,1,0:T(4,128)S(1)} %bitcast.28, bf16[256,2048]{1,0:T(8,128)(2,1)S(1)} %copy-done.4, f32[2048]{0:T(1024)S(1)} %copy-done.12, ...), kind=kOutput, calls=%fused_computation.9 | convolution fusion | flops 1078329344 | bytes 6835200 | tf_op jit(solution)/shard_map/dot_general | solution.py:30
  125.1 9.0 %reduce-scatter.3.cloned.1.call-done = bf16[256,1024]{1,0:T(8,128)(2,1)} async-done(((bf16[256,2048]{1,0:T(8,128)(2,1)}), bf16[256,1024]{1,0:T(8,128)(2,1)}) %reduce-scatter.3.cloned.1.call-update) | async-done | bytes 524304 | tf_op jit(solution)/shard_map/reduce_scatter | solution.py:97
  134.1 2.2 add_convert_fusion.1
  136.4 1.3 convert_element_type.77
  137.8 3.2 convert_element_type.78
  141.1 1.3 convert_element_type.80
  142.5 6.4 %all-gather.1 = f32[4,1,512]{2,1,0:T(1,128)S(1)} all-gather(f32[1,1,512]{2,1,0:T(1,128)S(1)} %bitcast.32), channel_id=1, replica_groups=mesh['rep'=4,'fs'=4,'tp'=2] {'fs'}, dimensions={0}, use_global_device_ids=true | all-gather | bytes 10240 | tf_op jit(solution)/shard_map/all_gather | solution.py:64
  148.9 1.5 fusion.7
  150.4 64.3 %all-gather.18.cloned.1.call-done = bf16[2048,1408]{1,0:T(8,128)(2,1)} async-done(((bf16[512,1408]{1,0:T(8,128)(2,1)}), bf16[2048,1408]{1,0:T(8,128)(2,1)}) %all-gather.18.cloned.1.call-update) | async-done | bytes 5767184 | tf_op jit(solution)/shard_map/all_gather | solution.py:20
  214.7 4.8 %convolution_multiply_fusion.1 = f32[256,1408]{1,0:T(8,128)S(1)} fusion(bf16[2048,1408]{1,0:T(8,128)(2,1)} %all-gather.18.cloned.1.call-done, f32[1408]{0:T(1024)S(1)} %copy-done.13, bf16[256,2048]{1,0:T(8,128)(2,1)} %all-gather.16.cloned.1.call-done, f32[2048]{0:T(1024)S(1)} %copy-done.14, f32[256]{0:T(256)S(1)} %add_rsqrt_fusion), kind=kOutput, calls=%fused_computation.2 | convolution fusion | flops 1478852608 | bytes 8272384 | tf_op jit(solution)/shard_map/dot_general | solution.py:24
  219.6 62.7 %all-gather.20.cloned.1.call-done = bf16[2048,1408]{1,0:T(8,128)(2,1)} async-done(((bf16[512,1408]{1,0:T(8,128)(2,1)}), bf16[2048,1408]{1,0:T(8,128)(2,1)}) %all-gather.20.cloned.1.call-update) | async-done | bytes 5767184 | tf_op jit(solution)/shard_map/all_gather | solution.py:21
  282.3 67.4 %all-gather.22.cloned.1.call-done = bf16[1408,2048]{1,0:T(8,128)(2,1)} async-done(((bf16[1408,512]{1,0:T(8,128)(2,1)}), bf16[1408,2048]{1,0:T(8,128)(2,1)}) %all-gather.22.cloned.1.call-update) | async-done | bytes 5767184 | tf_op jit(solution)/shard_map/all_gather | solution.py:32
  349.7 8.9 %fusion.2 = bf16[256,2048]{1,0:T(8,128)(2,1)} fusion(bf16[1408,2048]{1,0:T(8,128)(2,1)} %all-gather.22.cloned.1.call-done, f32[2048]{0:T(1024)S(1)} %bitcast.30, bf16[2048,1408]{1,0:T(8,128)(2,1)} %all-gather.20.cloned.1.call-done, f32[256,1408]{1,0:T(8,128)S(1)} %convolution_multiply_fusion.1, f32[1408]{0:T(1024)S(1)} %copy-done.15, ...), kind=kOutput, calls=%fused_computation.10 | convolution fusion | flops 2958458880 | bytes 15096320 | tf_op jit(solution)/shard_map/dot_general | solution.py:30
  358.6 9.1 %reduce-scatter.5.cloned.1.call-done = bf16[256,1024]{1,0:T(8,128)(2,1)} async-done(((bf16[256,2048]{1,0:T(8,128)(2,1)}), bf16[256,1024]{1,0:T(8,128)(2,1)}) %reduce-scatter.5.cloned.1.call-update) | async-done | bytes 524304 | tf_op jit(solution)/shard_map/reduce_scatter | solution.py:115
  367.7 2.0 add_convert_fusion
  (57 shorter events, 0.5 us)
Async XLA Ops:
  6.5 11.2 %copy-start = (f32[8,128]{1,0:T(8,128)S(1)}, f32[8,128]{1,0:T(8,128)}, u32[]{:S(2)}) copy-start(f32[8,128]{1,0:T(8,128)} %param.26) | copy-start | bytes 12292
  6.5 2.4 copy-start.5
  6.5 3.3 copy-start.6
  6.5 39.8 %all-gather.12.cloned.1.call-start = ((), (), s32[]{:S(2)}) async-start(), calls=%async_computation.3 | async-start | bytes 2621440 | tf_op jit(solution)/shard_map/all_gather | solution.py:21
  8.8 2.0 copy-start.10
  8.8 9.0 %copy-start.4 = (bf16[256,2048]{1,0:T(8,128)(2,1)S(1)}, bf16[256,2048]{1,0:T(8,128)(2,1)}, u32[]{:S(2)}) copy-start(bf16[256,2048]{1,0:T(8,128)(2,1)} %param.18) | copy-start | bytes 3145732
  8.8 74.5 %all-gather.10.cloned.1.call-start = ((), (), s32[]{:S(2)}) async-start(), calls=%async_computation.2 | async-start | bytes 2621440 | tf_op jit(solution)/shard_map/all_gather | solution.py:20
  9.8 36.5 %copy-start.12 = (f32[2048]{0:T(1024)S(1)}, f32[2048]{0:T(1024)}, u32[]{:S(2)}) copy-start(f32[2048]{0:T(1024)} %param.19) | copy-start | bytes 24580
  9.8 36.5 %copy-start.16 = (f32[512]{0:T(512)S(1)}, f32[512]{0:T(512)}, u32[]{:S(2)}) copy-start(f32[512]{0:T(512)} %param.23) | copy-start | bytes 6148
  9.8 110.4 %all-gather.14.cloned.1.call-start = ((), (), s32[]{:S(2)}) async-start(), calls=%async_computation.4 | async-start | bytes 2621440 | tf_op jit(solution)/shard_map/all_gather | solution.py:32
  10.8 123.4 %reduce-scatter.3.cloned.1.call-start = ((), (), s32[]{:S(2)}) async-start(), calls=%async_computation.5 | async-start | bytes 1572864 | tf_op jit(solution)/shard_map/reduce_scatter | solution.py:97
  18.1 33.8 %copy-start.9 = (f32[512]{0:T(512)S(1)}, f32[512]{0:T(512)}, u32[]{:S(2)}) copy-start(f32[512]{0:T(512)} %param.24) | copy-start | bytes 6148
  18.1 34.0 %copy-start.8 = (bf16[8,128,128]{2,1,0:T(8,128)(2,1)S(1)}, bf16[8,128,128]{2,1,0:T(8,128)(2,1)}, u32[]{:S(2)}) copy-start(bf16[8,128,128]{2,1,0:T(8,128)(2,1)} %param.25) | copy-start | bytes 786436
  48.9 71.4 %copy-start.17 = (f32[512]{0:T(512)S(1)}, f32[512]{0:T(512)}, u32[]{:S(2)}) copy-start(f32[512]{0:T(512)} %param.21) | copy-start | bytes 6148
  125.0 11.3 %copy-start.2 = (f32[512,1408]{1,0:T(8,128)S(1)}, f32[512,1408]{1,0:T(8,128)}, u32[]{:S(2)}) copy-start(f32[512,1408]{1,0:T(8,128)} %param.30) | copy-start | bytes 8650756
  125.1 23.8 %all-gather.16.cloned.1.call-start = ((), (), s32[]{:S(2)}) async-start(), calls=%async_computation.6 | async-start | bytes 1572864 | tf_op jit(solution)/shard_map/all_gather | solution.py:104
  136.3 78.4 %all-gather.18.cloned.1.call-start = ((), (), s32[]{:S(2)}) async-start(), calls=%async_computation.7 | async-start | bytes 7208960 | tf_op jit(solution)/shard_map/all_gather | solution.py:20
  137.7 3.4 copy-start.3
  137.7 144.6 %all-gather.20.cloned.1.call-start = ((), (), s32[]{:S(2)}) async-start(), calls=%async_computation.8 | async-start | bytes 7208960 | tf_op jit(solution)/shard_map/all_gather | solution.py:21
  141.0 1.5 copy-start.11
  141.0 208.6 %all-gather.22.cloned.1.call-start = ((), (), s32[]{:S(2)}) async-start(), calls=%async_computation.9 | async-start | bytes 7208960 | tf_op jit(solution)/shard_map/all_gather | solution.py:32
  142.4 72.3 %copy-start.13 = (f32[1408]{0:T(1024)S(1)}, f32[1408]{0:T(1024)}, u32[]{:S(2)}) copy-start(f32[1408]{0:T(1024)} %param.31) | copy-start | bytes 16900
  142.4 72.3 %copy-start.14 = (f32[2048]{0:T(1024)S(1)}, f32[2048]{0:T(1024)}, u32[]{:S(2)}) copy-start(f32[2048]{0:T(1024)} %param.29) | copy-start | bytes 24580
  142.4 225.3 %reduce-scatter.5.cloned.1.call-start = ((), (), s32[]{:S(2)}) async-start(), calls=%async_computation.10 | async-start | bytes 1572864 | tf_op jit(solution)/shard_map/reduce_scatter | solution.py:115
  150.4 199.3 %copy-start.7 = (bf16[256,2048]{1,0:T(8,128)(2,1)S(1)}, bf16[256,2048]{1,0:T(8,128)(2,1)}, u32[]{:S(2)}) copy-start(bf16[256,2048]{1,0:T(8,128)(2,1)} %all-gather.16.cloned.1.call-done) | copy-start | bytes 3145732
  150.4 199.3 %copy-start.15 = (f32[1408]{0:T(1024)S(1)}, f32[1408]{0:T(1024)}, u32[]{:S(2)}) copy-start(f32[1408]{0:T(1024)} %param.33) | copy-start | bytes 16900
  349.7 18.1 %copy-start.1 = (bf16[256,1024]{1,0:T(8,128)(2,1)S(1)}, bf16[256,1024]{1,0:T(8,128)(2,1)}, u32[]{:S(2)}) copy-start(bf16[256,1024]{1,0:T(8,128)(2,1)} %add_convert_fusion.1) | copy-start | bytes 1572868
Sparse Core Ops, SparseCore 0:
  9.2 37.0 all-gather.11
  48.1 35.1 all-gather.9
  85.2 35.0 all-gather.13
  125.2 8.8 reduce-scatter.2
  136.5 10.2 all-gather.15
  148.4 66.2 all-gather.17
  216.6 65.6 all-gather.19
  284.1 65.5 all-gather.21
  358.8 8.9 reduce-scatter.4
where the time goes:
time: 377 us; the launch traced here: 376 us
  waiting for transfers between devices  309 us (82%)
  matrix products  21.4 us (6%)
  blocking collectives  16.2 us (4%)
  other arithmetic  16 us (4%)
  between operations  13.4 us (4%)
    all_gather x2, waiting for transfers between devices, collect_cols(): lax.all_gather(shard_rows, 'fs', axis=1, tiled=True)  104 us
    all_gather x2, waiting for transfers between devices, assembled_entries(): lax.all_gather(pieces[0], 'fs', axis=0, tiled=True)  95.1 us
    all_gather x2, waiting for transfers between devices, assembled_entries(): lax.all_gather(pieces[1], 'fs', axis=0, tiled=True)  90.9 us
    dot_general x2, matrix products, collect_cols(): jnp.dot(activations, lax.all_gather(shard_rows, 'fs', axis=1, tiled=True)...  13.7 us
    reduce_scatter x1, waiting for transfers between devices, on_device(): lax.psum_scatter(ffn_terms.astype(jnp.bfloat16), 'tp', scatter_dimension=...  9.08 us
    reduce_scatter x1, waiting for transfers between devices, on_device(): lax.psum_scatter(mix_terms.astype(jnp.bfloat16), 'tp', scatter_dimension=...  9 us
  transfers between devices with their start and end apart: 9, of which 8 were waited for; matrix products, arithmetic and copies ran while one was open for 5% of the time, Pallas kernels for 0%

commit v1 on v0

v1 whole, which is shorter than its diff:
```python
import jax
import jax.numpy as jnp
from jax import lax
from jax.sharding import PartitionSpec as P

BLENDER_FEATURES = 1024
GROUP_DIM = 128
BLOCK = 128


epsilon = 1e-06


def normalize(values, gain):
    return values * lax.rsqrt(jnp.mean(values * values, axis=-1, keepdims=True) + epsilon) * gain


def on_device(
    skip_stream_entry,
    sequence_blender_factor,
    product_projector,
    product_side_factors,
    placewise_projector,
    placewise_entry_factors,
    placewise_rescale_factor,
    place_cluster_operator,
    placewise_offset_vector,
    blender_result_projector,
    blender_result_factors,
    feedforward_norm_factor,
    switch_projector,
    switch_factors,
    expand_projector,
    expand_factors,
    contract_projector,
    contract_factors,
):
    rep = lax.axis_size("rep")
    tp = lax.axis_size("tp")
    rep_index = lax.axis_index("rep")
    tp_index = lax.axis_index("tp")
    group = ("rep", "tp")
    steps, embed = skip_stream_entry.shape
    own_steps = steps // tp
    own_features = embed // tp
    channels = product_projector.shape[1] // rep
    hidden = switch_projector.shape[1] // rep

    def part(values, size, dim):
        return lax.dynamic_slice_in_dim(values, rep_index * size, size, dim)

    def gathered(first, second, out, size):
        return lax.all_gather(
            jnp.concatenate(
                (
                    part(first, size, 1).astype(jnp.bfloat16),
                    part(second, size, 1).astype(jnp.bfloat16),
                    part(out, size, 0).astype(jnp.bfloat16).T,
                ),
                axis=1,
            ),
            "fs",
            axis=0,
            tiled=True,
        )

    own_entry = lax.dynamic_slice_in_dim(skip_stream_entry, tp_index * own_steps, own_steps, 0)
    normed = lax.all_gather(
        normalize(own_entry.astype(jnp.float32), sequence_blender_factor).astype(jnp.bfloat16),
        group,
        axis=0,
        tiled=True,
    )
    mixer_weights = gathered(
        product_projector, placewise_projector, blender_result_projector, channels
    )
    out_scales = lax.all_gather(
        jnp.stack((blender_result_factors, contract_factors)), "fs", axis=1, tiled=True
    )
    ffn_weights = gathered(switch_projector, expand_projector, contract_projector, hidden)

    tokens = normed.shape[0]
    plain = jnp.dot(normed, mixer_weights[:, : 2 * channels], preferred_element_type=jnp.float32)
    carrier = jax.nn.gelu(plain[:, :channels] * part(product_side_factors, channels, 0))
    spread = jax.nn.gelu(plain[:, channels:] * part(placewise_entry_factors, channels, 0))
    squares = lax.psum(jnp.sum(spread * spread, axis=1), group)
    factor = lax.rsqrt(squares / BLENDER_FEATURES + epsilon)
    spread_normed = (
        spread * factor[:, None] * part(placewise_rescale_factor, channels, 0)
    ).astype(jnp.bfloat16)
    span = min(channels, GROUP_DIM)
    count = max(1, channels // GROUP_DIM)
    first_group = (tp_index * rep + rep_index) * channels // GROUP_DIM
    causal = jnp.tril(jnp.ones((BLOCK, BLOCK), dtype=bool))
    local_weight = lax.dynamic_slice_in_dim(place_cluster_operator, first_group, count, 0)
    local_weight = jnp.where(causal[None], local_weight, jnp.zeros_like(local_weight))
    local_bias = lax.dynamic_slice_in_dim(placewise_offset_vector, first_group, count, 0)
    blocks = spread_normed.reshape(tokens // BLOCK, BLOCK, count, span)
    mixed = jnp.einsum("gts,nsgc->ntgc", local_weight, blocks, preferred_element_type=jnp.float32)
    mixed = mixed + local_bias.T[None, :, :, None]
    gated = (carrier * mixed.reshape(tokens, channels)).astype(jnp.bfloat16)

    def projected(values, weights, scales):
        return (
            lax.dot_general(
                values, weights, (((1,), (1,)), ((), ())), preferred_element_type=jnp.float32
            )
            * scales
        ).astype(jnp.bfloat16)

    mix_total = lax.psum_scatter(
        projected(gated, mixer_weights[:, 2 * channels :], out_scales[0]),
        group,
        scatter_dimension=0,
        tiled=True,
    )
    stream = (own_entry.astype(jnp.float32) + mix_total.astype(jnp.float32)).astype(jnp.bfloat16)
    stream_all = lax.all_gather(stream, group, axis=0, tiled=True)
    ffn_normed = normalize(stream_all.astype(jnp.float32), feedforward_norm_factor).astype(
        jnp.bfloat16
    )
    plain = jnp.dot(ffn_normed, ffn_weights[:, : 2 * hidden], preferred_element_type=jnp.float32)
    active = (
        jax.nn.silu(plain[:, :hidden] * part(switch_factors, hidden, 0))
        * (plain[:, hidden:] * part(expand_factors, hidden, 0))
    ).astype(jnp.bfloat16)
    ffn_terms = projected(active, ffn_weights[:, 2 * hidden :], out_scales[1])
    ffn_terms = ffn_terms.reshape(rep, steps, tp, own_features).transpose(0, 2, 1, 3)
    ffn_total = lax.psum_scatter(
        ffn_terms.reshape(rep * tp * steps, own_features), group, scatter_dimension=0, tiled=True
    )
    own_stream = lax.dynamic_slice(
        stream_all, (rep_index * steps, tp_index * own_features), (steps, own_features)
    )
    return (own_stream.astype(jnp.float32) + ffn_total.astype(jnp.float32)).astype(jnp.bfloat16)


def solution(mesh):
    return jax.shard_map(
        on_device,
        mesh=mesh,
        in_specs=(
            P(("rep", "fs"), None),
            P(),
            P("fs", "tp"),
            P("tp"),
            P("fs", "tp"),
            P("tp"),
            P("tp"),
            P(),
            P(),
            P("tp", "fs"),
            P("fs"),
            P(),
            P("fs", "tp"),
            P("tp"),
            P("fs", "tp"),
            P("tp"),
            P("tp", "fs"),
            P("fs"),
        ),
        out_specs=P(("rep", "fs"), "tp"),
        check_vma=False,
    )
```

time: 377 us -> 355 us (0.942)
  waiting for transfers between devices: 309 us -> 253 us
  local copies, waits for them, and re-layouts: 0.39 us -> 26.6 us
  blocking collectives: 16.2 us -> 20.2 us
    all_gather x7 -> x4, waiting for transfers between devices: 290 us -> 157 us  [the longest x2 69.8 us: gathered(): lax.all_gather(jnp.concatenate((part(first, size, 1).astype(jnp.bfloat16)...]
    reduce_scatter x2, waiting for transfers between devices: 18.1 us -> 95.6 us  [the longest x1 48.3 us: on_device(): lax.psum_scatter(ffn_terms.reshape(rep * tp * steps, own_features), group...]
    reshape x1 -> x2, local copies, waits for them, and re-layouts: 0.07 us -> 13.3 us  [on_device(): ffn_terms.reshape(rep, steps, tp, own_features).transpose(0, 2, 1, 3)]
    psum x1, blocking collectives: 2.97 us -> 13.2 us  [on_device(): squares = lax.psum(jnp.sum(spread * spread, axis=1), group)]
    dynamic_slice x0 -> x7, local copies, waits for them, and re-layouts: none -> 7.49 us  [part(): return lax.dynamic_slice_in_dim(values, rep_index * size, size, dim)]
    all_gather x2 -> x1, blocking collectives: 13.3 us -> 6.99 us  [on_device(): lax.all_gather(jnp.stack((blender_result_factors, contract_factors)), 'fs...]
    convert_element_type x9 -> x5, other arithmetic: 14.1 us -> 8.87 us  [the longest x1 2.19 us: on_device(): (own_stream.astype(jnp.float32) + ffn_total.astype(jnp.float32)).astype(j...]
    unnamed x36 -> x16, local copies, waits for them, and re-layouts: 0.09 us -> 4.02 us
  transfers between devices with their start and end apart: 9 -> 6, of which waited for: 8 -> 6; matrix products, arithmetic and copies ran while one was open for 5% -> 5% of each run, Pallas kernels for 0% -> 0%
where the time goes in v1:
time: 355 us; the launch traced here: 351 us
  waiting for transfers between devices  253 us (71%)
  local copies, waits for them, and re-layouts  26.6 us (7%)
  matrix products  21.2 us (6%)
  blocking collectives  20.2 us (6%)
  other arithmetic  16.5 us (5%)
  between operations  13.6 us (4%)
    all_gather x2, waiting for transfers between devices, gathered(): lax.all_gather(jnp.concatenate((part(first, size, 1).astype(jnp.bfloat16)...  69.8 us
    all_gather x1, waiting for transfers between devices, on_device(): lax.all_gather(normalize(own_entry.astype(jnp.float32), sequence_blender_...  49.1 us
    reduce_scatter x1, waiting for transfers between devices, on_device(): lax.psum_scatter(ffn_terms.reshape(rep * tp * steps, own_features), group...  48.3 us
    reduce_scatter x1, waiting for transfers between devices, on_device(): lax.psum_scatter(projected(gated, mixer_weights[:, 2 * channels:], out_sc...  47.2 us
    all_gather x1, waiting for transfers between devices, on_device(): stream_all = lax.all_gather(stream, group, axis=0, tiled=True)  38.2 us
    reshape x2, local copies, waits for them, and re-layouts, on_device(): ffn_terms.reshape(rep, steps, tp, own_features).transpose(0, 2, 1, 3)  13.3 us
    psum x1, blocking collectives, on_device(): squares = lax.psum(jnp.sum(spread * spread, axis=1), group)  13.2 us
    dot_general x2, matrix products, projected(): lax.dot_general(values, weights, (((1,), (1,)), ((), ())), preferred_elem...  10.2 us
  transfers between devices with their start and end apart: 6, of which 6 were waited for; matrix products, arithmetic and copies ran while one was open for 5% of the time, Pallas kernels for 0%

profile of v1, /device:TPU:1, one launch (start us, length us, event | category | flops | bytes accessed | tf_op | source)
XLA Modules:
  0.0 351.4 jit_solution(6940067119507014527)
XLA Ops:
  6.6 1.1 fusion.40
  7.7 1.1 constant_dynamic-slice_fusion.3
  9.0 0.8 pad_maximum_fusion.1
  9.9 1.2 fusion.12
  11.2 2.0 fusion.14
  15.6 7.0 %all_gather.17 = f32[2,2048]{1,0:T(2,128)S(1)} all-gather(f32[2,512]{1,0:T(2,128)S(1)} %pad_maximum_fusion.2), channel_id=1, replica_groups=mesh['rep'=4,'fs'=4,'tp'=2] {'fs'}, dimensions={1}, use_global_device_ids=true | all-gather | bytes 20480 | tf_op jit(solution)/shard_map/all_gather | solution.py:77
  23.3 19.4 %all-gather.7.cloned.1.call-done = bf16[2048,384]{0,1:T(8,128)(2,1)} async-done(((bf16[512,384]{0,1:T(8,128)(2,1)}), bf16[2048,384]{0,1:T(8,128)(2,1)}) %all-gather.7.cloned.1.call-update) | async-done | bytes 1572880 | tf_op jit(solution)/shard_map/all_gather | solution.py:53
  42.6 49.1 %all-gather.5.cloned.1.call-done = bf16[1024,2048]{1,0:T(8,128)(2,1)} async-done(((bf16[128,2048]{1,0:T(8,128)(2,1)}), bf16[1024,2048]{1,0:T(8,128)(2,1)}) %all-gather.5.cloned.1.call-update) | async-done | bytes 4194320 | tf_op jit(solution)/shard_map/all_gather | solution.py:68
  91.7 3.8 %fusion.16 = f32[1024,256]{1,0:T(8,128)S(1)} fusion(bf16[1024,2048]{1,0:T(8,128)(2,1)} %all-gather.5.cloned.1.call-done, bf16[2048,384]{0,1:T(8,128)(2,1)} %all-gather.7.cloned.1.call-done), kind=kOutput, calls=%fused_computation.26 | convolution fusion | flops 1073741824 | bytes 6291456 | tf_op jit(solution)/shard_map/dot_general | solution.py:83
  95.5 1.0 copy-done.1
  96.7 13.2 %psum.7 = f32[1024]{0:T(1024)S(1)} all-reduce(f32[1024]{0:T(1024)S(1)} %multiply_reduce_fusion), channel_id=1, replica_groups=mesh['rep'=4,'fs'=4,'tp'=2] {'rep','tp'}, use_global_device_ids=true, to_apply=%region_2.0 | all-reduce | flops 1024 | bytes 8192 | tf_op jit(solution)/shard_map/psum | solution.py:86
  110.0 1.3 multiply_convert_fusion.2
  111.2 1.0 fusion.11
  112.2 1.3 fusion.30
  113.5 4.2 %multiply_convert_fusion.1 = bf16[1024,2048]{1,0:T(8,128)(2,1)} fusion(bf16[1024,128]{1,0:T(8,128)(2,1)S(1)} %fusion.30, f32[2048]{0:T(1024)S(1)} %bitcast.31, bf16[2048,384]{0,1:T(8,128)(2,1)} %all-gather.7.cloned.1.call-done), kind=kOutput, calls=%fused_computation.6 | convolution fusion | flops 541065216 | bytes 4988928 | tf_op jit(solution)/shard_map/dot_general | solution.py:105
  117.8 47.2 %reduce-scatter.3.cloned.1.call-done = bf16[128,2048]{1,0:T(8,128)(2,1)} async-done(((bf16[1024,2048]{1,0:T(8,128)(2,1)}), bf16[128,2048]{1,0:T(8,128)(2,1)}) %reduce-scatter.3.cloned.1.call-update) | async-done | bytes 524304 | tf_op jit(solution)/shard_map/reduce_scatter | solution.py:111
  165.0 2.1 fusion.15
  167.2 2.6 constant_dynamic-slice_fusion
  169.8 1.9 copy.27
  171.7 0.9 copy.26
  172.7 2.2 pad_maximum_fusion
  175.2 0.8 dynamic_slice.58
  176.0 0.8 dynamic_slice.59
  176.8 38.2 %all-gather.9.cloned.1.call-done = bf16[1024,2048]{1,0:T(8,128)(2,1)} async-done(((bf16[128,2048]{1,0:T(8,128)(2,1)}), bf16[1024,2048]{1,0:T(8,128)(2,1)}) %all-gather.9.cloned.1.call-update) | async-done | bytes 4194320 | tf_op jit(solution)/shard_map/all_gather | solution.py:118
  214.9 3.1 fusion
  218.0 50.4 %all-gather.11.cloned.1.call-done = bf16[2048,1056]{0,1:T(8,128)(2,1)} async-done(((bf16[512,1056]{0,1:T(8,128)(2,1)}), bf16[2048,1056]{0,1:T(8,128)(2,1)}) %all-gather.11.cloned.1.call-update) | async-done | bytes 4325392 | tf_op jit(solution)/shard_map/all_gather | solution.py:53
  268.5 6.3 %fusion.3 = f32[1024,704]{0,1:T(8,128)S(1)} fusion(bf16[1024,2048]{1,0:T(8,128)(2,1)} %all-gather.9.cloned.1.call-done, f32[2048]{0:T(1024)S(1)} %copy-done.5, f32[1024]{0:T(1024)S(1)} %add_rsqrt_fusion, bf16[2048,1056]{0,1:T(8,128)(2,1)} %all-gather.11.cloned.1.call-done), kind=kOutput, calls=%fused_computation.7 | convolution fusion | flops 2961178624 | bytes 9973760 | tf_op jit(solution)/shard_map/dot_general | solution.py:122
  274.8 6.0 %multiply_convert_fusion = bf16[1024,2048]{1,0:T(8,128)(2,1)} fusion(f32[2048]{0:T(1024)S(1)} %bitcast.32, bf16[2048,1056]{0,1:T(8,128)(2,1)} %all-gather.11.cloned.1.call-done, f32[1024,704]{0,1:T(8,128)S(1)} %fusion.3, f32[352]{0:T(512)S(1)} %dynamic_slice.59, f32[352]{0:T(512)S(1)} %dynamic_slice.58), kind=kOutput, calls=%fused_computation.5 | convolution fusion | flops 1483472896 | bytes 8530688 | tf_op jit(solution)/shard_map/dot_general | solution.py:105
  280.7 7.8 %reshape.59 = bf16[4,256,2,1024]{3,2,1,0:T(2,128)(2,1)} reshape(bf16[1024,2048]{1,0:T(8,128)(2,1)} %multiply_convert_fusion) | data formatting | bytes 8388608 | tf_op jit(solution)/shard_map/reshape | solution.py:128
  288.5 5.5 %copy.23 = bf16[4,256,2,1024]{3,1,2,0:T(8,128)(2,1)} copy(bf16[4,256,2,1024]{3,2,1,0:T(2,128)(2,1)} %reshape.59) | data formatting | bytes 8388608 | tf_op jit(solution)/shard_map/reshape | solution.py:128
  294.0 48.3 %reduce-scatter.5.cloned.1.call-done = bf16[256,1024]{1,0:T(8,128)(2,1)} async-done(((bf16[2048,1024]{1,0:T(8,128)(2,1)}), bf16[256,1024]{1,0:T(8,128)(2,1)}) %reduce-scatter.5.cloned.1.call-update) | async-done | bytes 524304 | tf_op jit(solution)/shard_map/reduce_scatter | solution.py:129
  342.4 2.2 add_convert_fusion
  (36 shorter events, 4.1 us)
Async XLA Ops:
  6.5 166.1 %copy-start = (f32[1408,512]{1,0:T(8,128)S(1)}, f32[1408,512]{1,0:T(8,128)}, u32[]{:S(2)}) copy-start(f32[1408,512]{1,0:T(8,128)} %param.34) | copy-start | bytes 8650756
  6.5 4.6 %copy-start.2 = (f32[2048]{0:T(1024)S(1)}, f32[2048]{0:T(1024)}, u32[]{:S(2)}) copy-start(f32[2048]{0:T(1024)} %param.19) | copy-start | bytes 24580
  6.5 9.0 %copy-start.3 = (f32[512]{0:T(512)S(1)}, f32[512]{0:T(512)}, u32[]{:S(2)}) copy-start(f32[512]{0:T(512)} %param.35) | copy-start | bytes 6148
  6.5 9.0 %copy-start.4 = (f32[512]{0:T(512)S(1)}, f32[512]{0:T(512)}, u32[]{:S(2)}) copy-start(f32[512]{0:T(512)} %param.28) | copy-start | bytes 6148
  6.5 36.1 %all-gather.7.cloned.1.call-start = ((), (), s32[]{:S(2)}) async-start(), calls=%async_computation.3 | async-start | bytes 1966080 | tf_op jit(solution)/shard_map/all_gather | solution.py:53
  9.8 81.8 %all-gather.5.cloned.1.call-start = ((), (), s32[]{:S(2)}) async-start(), calls=%async_computation.2 | async-start | bytes 4718592 | tf_op jit(solution)/shard_map/all_gather | solution.py:68
  13.2 151.8 %reduce-scatter.3.cloned.1.call-start = ((), (), s32[]{:S(2)}) async-start(), calls=%async_computation.4 | async-start | bytes 4718592 | tf_op jit(solution)/shard_map/reduce_scatter | solution.py:111
  95.5 1.0 copy-start.1
  117.8 97.2 %all-gather.9.cloned.1.call-start = ((), (), s32[]{:S(2)}) async-start(), calls=%async_computation.5 | async-start | bytes 4718592 | tf_op jit(solution)/shard_map/all_gather | solution.py:118
  167.2 101.3 %all-gather.11.cloned.1.call-start = ((), (), s32[]{:S(2)}) async-start(), calls=%async_computation.6 | async-start | bytes 5406720 | tf_op jit(solution)/shard_map/all_gather | solution.py:53
  174.9 93.5 %copy-start.5 = (f32[2048]{0:T(1024)S(1)}, f32[2048]{0:T(1024)}, u32[]{:S(2)}) copy-start(f32[2048]{0:T(1024)} %param.29) | copy-start | bytes 24580
  175.0 167.4 %reduce-scatter.5.cloned.1.call-start = ((), (), s32[]{:S(2)}) async-start(), calls=%async_computation.7 | async-start | bytes 4718592 | tf_op jit(solution)/shard_map/reduce_scatter | solution.py:129
Sparse Core Ops, SparseCore 0:
  10.0 32.6 all-gather.6
  44.2 47.4 all-gather.4
  117.9 47.1 reduce-scatter.2
  167.3 47.5 all-gather.8
  216.6 51.8 all-gather.10
  294.1 48.1 reduce-scatter.4

commit v2 on v1

--- a/solution.py
+++ b/solution.py
@@ -1,6 +1,10 @@
+import functools
+
 import jax
 import jax.numpy as jnp
 from jax import lax
+from jax.experimental import pallas as pl
+from jax.experimental.pallas import tpu as pltpu
 from jax.sharding import PartitionSpec as P
 
 BLENDER_FEATURES = 1024
@@ -15,7 +19,7 @@
     return values * lax.rsqrt(jnp.mean(values * values, axis=-1, keepdims=True) + epsilon) * gain
 
 
-def on_device(
+def with_collectives(
     skip_stream_entry,
     sequence_blender_factor,
     product_projector,
@@ -135,6 +139,497 @@
     return (own_stream.astype(jnp.float32) + ffn_total.astype(jnp.float32)).astype(jnp.bfloat16)
 
 
+MESH = pl.DeviceIdType.MESH
+F32 = jnp.float32
+BF16 = jnp.bfloat16
+RIGHT = (((1,), (0,)), ((), ()))
+
+
+def dot(a, b):
+    return lax.dot_general(a, b, RIGHT, preferred_element_type=F32)
+
+
+def layer_kernel(
+    x_ref,
+    wm_ref,
+    wb_ref,
+    wg_ref,
+    wc_ref,
+    sc_ref,
+    gain_ref,
+    ffn_gain_ref,
+    mixer_scale_ref,
+    rescale_ref,
+    ffn_scale_ref,
+    place_ref,
+    bias_ref,
+    out_ref,
+    wm_in,
+    wb_in,
+    wg_in,
+    wc_in,
+    sc_in,
+    x_in,
+    xn,
+    carrier,
+    spread,
+    gated,
+    sums,
+    sums_in,
+    parts,
+    core_in,
+    pair_out,
+    pair_in,
+    stream,
+    active,
+    ffn_parts,
+    ffn_core_in,
+    ffn_pair_out,
+    ffn_pair_in,
+    send_w,
+    recv_w,
+    send_sc,
+    recv_sc,
+    send_a,
+    recv_a,
+    mixer_channels,
+    all_channels,
+):
+    r = lax.axis_index("rep")
+    f = lax.axis_index("fs")
+    k = lax.axis_index("tp")
+    fx, fy = f % 2, f // 2
+    seat = (f, fy * 2 + 1 - fx, (1 - fy) * 2 + fx, 3 - f)
+    to_x, to_y, to_d = {"fs": seat[1]}, {"fs": seat[2]}, {"fs": seat[3]}
+    to_pair = {"rep": r + 1 - 2 * (r % 2)}
+    to_core = {"tp": 1 - k}
+    steps = x_ref.shape[0]
+    tokens = 2 * steps
+    width = wm_ref.shape[0]
+
+    barrier = pltpu.get_barrier_semaphore()
+    for other in (to_x, to_y, to_d, to_pair, to_core):
+        pl.semaphore_signal(barrier, inc=1, device_id=other, device_id_type=MESH)
+    pl.semaphore_wait(barrier, 5)
+
+    def remote(src, dst, send, recv, device):
+        return pltpu.make_async_remote_copy(
+            src_ref=src, dst_ref=dst, send_sem=send, recv_sem=recv,
+            device_id=device, device_id_type=MESH,
+        )
+
+    pieces = []
+    for ref, buf, n in ((wm_ref, wm_in, 2), (wb_ref, wb_in, 1), (wg_ref, wg_in, 4), (wc_ref, wc_in, 2)):
+        size = ref.shape[0] // n
+        for i in range(n):
+            pieces.append((ref, buf, i * size, size))
+
+    def own(i):
+        ref, buf, start, size = pieces[i]
+        rows = pl.ds(start, size)
+        return (
+            remote(ref.at[rows], buf.at[0, rows], send_w.at[i, 0], recv_w.at[i, 0], to_x),
+            remote(ref.at[rows], buf.at[1, rows], send_w.at[i, 1], recv_w.at[i, 1], to_y),
+        )
+
+    def onward(i):
+        ref, buf, start, size = pieces[i]
+        first, last = pl.ds(start, size // 2), pl.ds(start + size // 2, size // 2)
+        return (
+            remote(buf.at[0, first], buf.at[2, first], send_w.at[i, 2], recv_w.at[i, 2], to_y),
+            remote(buf.at[1, last], buf.at[2, last], send_w.at[i, 3], recv_w.at[i, 3], to_x),
+        )
+
+    def issue(i):
+        if i < len(pieces):
+            for copy in own(i):
+                copy.start()
+
+    def step(i, ahead):
+        for copy in own(i):
+            copy.wait_recv()
+        for copy in onward(i):
+            copy.start()
+        issue(i + ahead)
+
+    def far(i):
+        for copy in onward(i):
+            copy.wait_recv()
+
+    scale_copies = [
+        remote(sc_ref, sc_in.at[s], send_sc.at[s], recv_sc.at[s], device)
+        for s, device in enumerate((to_x, to_y, to_d))
+    ]
+    x_copy = remote(x_ref, x_in, send_a.at[0], recv_a.at[0], to_pair)
+    for copy in scale_copies:
+        copy.start()
+    issue(0)
+    x_copy.start()
+    issue(1)
+
+    def feature(s):
+        return pl.ds(pl.multiple_of(seat[s] * width, width), width)
+
+    def norm_tile(load, gain, row, size):
+        values = [load(s, row).astype(F32) for s in range(4)]
+        total = sum(jnp.sum(v * v, axis=1, keepdims=True) for v in values)
+        inverse = lax.rsqrt(total / (4 * width) + epsilon)
+        for s in range(4):
+            xn[s, pl.ds(row, size), :] = (values[s] * inverse * gain[:, feature(s)]).astype(BF16)
+
+    tile = 64
+
+    def norm_own(i, carry):
+        norm_tile(lambda s, row: x_ref[pl.ds(row, tile), feature(s)], gain_ref, i * tile, tile)
+        return carry
+
+    lax.fori_loop(0, steps // tile, norm_own, 0)
+    step(0, 2)
+    step(1, 2)
+    x_copy.wait_recv()
+
+    def norm_pair(i, carry):
+        norm_tile(
+            lambda s, row: x_in[pl.ds(i * tile, tile), feature(s)],
+            gain_ref, steps + i * tile, tile,
+        )
+        return carry
+
+    lax.fori_loop(0, steps // tile, norm_pair, 0)
+    far(0)
+    far(1)
+
+    half = 256
+    mixer_in = (wm_ref, wm_in.at[0], wm_in.at[1], wm_in.at[2])
+
+    def mixer_rows(i, carry):
+        rows = pl.ds(pl.multiple_of(i * half, half), half)
+        plain = dot(xn[0, rows, :], mixer_in[0][...])
+        for s in range(1, 4):
+            plain += dot(xn[s, rows, :], mixer_in[s][...])
+        both = jax.nn.gelu(plain * mixer_scale_ref[...])
+        carrier[rows, :] = both[:, :mixer_channels]
+        own_spread = both[:, mixer_channels:]
+        spread[rows, :] = own_spread
+        total = jnp.sum(own_spread * own_spread, axis=1, keepdims=True)
+        sums[0, :, rows] = jnp.broadcast_to(total, (half, 128)).T[:8]
+        return carry
+
+    lax.fori_loop(0, tokens // half, mixer_rows, 0)
+    core_sums = remote(sums.at[0], sums_in.at[0], send_a.at[1], recv_a.at[1], to_core)
+    core_sums.start()
+    core_sums.wait_recv()
+    sums[1] = sums[0] + sums_in[0]
+    pair_sums = remote(sums.at[1], sums_in.at[1], send_a.at[2], recv_a.at[2], to_pair)
+    pair_sums.start()
+    step(2, 2)
+    pair_sums.wait_recv()
+    received = sums_in[1]
+    received = jnp.concatenate((received[:, steps:], received[:, :steps]), axis=1)
+    sums[2] = lax.rsqrt((sums[1] + received) / all_channels + epsilon)
+
+    def mix_rows(i, carry):
+        rows = pl.ds(pl.multiple_of(i * BLOCK, BLOCK), BLOCK)
+        factor = jnp.concatenate([sums[2, :, rows]] * (128 // 8), axis=0).T[:, :1]
+        normed = (spread[rows, :] * factor * rescale_ref[...]).astype(BF16)
+        for g in range(mixer_channels // GROUP_DIM):
+            lanes = pl.ds(g * GROUP_DIM, GROUP_DIM)
+            mixed = dot(place_ref[g], normed[:, g * GROUP_DIM : (g + 1) * GROUP_DIM])
+            mixed = mixed + bias_ref[:, lanes]
+            gated[rows, lanes] = (carrier[rows, lanes] * mixed).astype(BF16)
+        return carry
+
+    lax.fori_loop(0, tokens // BLOCK, mix_rows, 0)
+    for copy in scale_copies:
+        copy.wait_recv()
+    scales = (sc_ref, sc_in.at[0], sc_in.at[1], sc_in.at[2])
+    keep = (k + fy) % 2
+    base = 2 * keep
+
+    def project(values, weights, row, s, target):
+        def rows_of(i, carry):
+            rows = pl.ds(pl.multiple_of(i * half, half), half)
+            target[s, rows, :] = (
+                dot(values[rows, :], weights[...]) * scales[s][row : row + 1, :]
+            ).astype(BF16)
+            return carry
+
+        lax.fori_loop(0, tokens // half, rows_of, 0)
+
+    mixer_out = (wb_ref, wb_in.at[0], wb_in.at[1], wb_in.at[2])
+    ffn_out = (wc_ref, wc_in.at[0], wc_in.at[1], wc_in.at[2])
+
+    give = pl.ds(2 - base, 2)
+    mix_give = remote(parts.at[give], core_in, send_a.at[3], recv_a.at[3], to_core)
+    mix_pair = [
+        remote(pair_out.at[j], pair_in.at[j], send_a.at[4 + j], recv_a.at[4 + j], to_pair)
+        for j in range(2)
+    ]
+
+    def merge_mix():
+        mix_give.wait_recv()
+        for j in range(2):
+            def rows_of(i, carry):
+                rows = pl.ds(pl.multiple_of(i * half, half), half)
+                pair_out[j, rows, :] = (
+                    parts[base + j, rows, :].astype(F32) + core_in[j, rows, :].astype(F32)
+                ).astype(BF16)
+                return carry
+
+            lax.fori_loop(0, tokens // half, rows_of, 0)
+            mix_pair[j].start()
+
+    for t in range(2):
+        if t == 1:
+            far(2)
+        for s in (2 * t, 2 * t + 1):
+            project(gated, mixer_out[s], 0, s, parts)
+
+        @pl.when(keep != t)
+        def _():
+            mix_give.start()
+
+        @pl.when(keep == t)
+        def _():
+            merge_mix()
+
+    step(3, 2)
+    step(4, 2)
+
+    stream_give = [
+        remote(stream.at[base + j], stream.at[base + j], send_a.at[6 + j], recv_a.at[6 + j], to_core)
+        for j in range(2)
+    ]
+    stream_take = [
+        remote(stream.at[2 - base + j], stream.at[2 - base + j], send_a.at[6 + j], recv_a.at[6 + j], to_core)
+        for j in range(2)
+    ]
+    block_of = (seat[0] + keep * (seat[2] - seat[0]), seat[1] + keep * (seat[3] - seat[1]))
+    for j in range(2):
+        mix_pair[j].wait_recv()
+        lanes = pl.ds(pl.multiple_of(block_of[j] * width, width), width)
+        for first, second, source in ((0, steps, x_ref), (steps, 0, x_in)):
+            rows = pl.ds(first, steps)
+            stream[base + j, rows, :] = (
+                source[:, lanes].astype(F32)
+                + (
+                    pair_out[j, rows, :].astype(F32)
+                    + pair_in[j, pl.ds(second, steps), :].astype(F32)
+                )
+            ).astype(BF16)
+        stream_give[j].start()
+    for copy in stream_take:
+        copy.wait_recv()
+
+    def norm_stream(i, carry):
+        norm_tile(
+            lambda s, row: stream[s, pl.ds(row, tile), :], ffn_gain_ref, i * tile, tile
+        )
+        return carry
+
+    lax.fori_loop(0, tokens // tile, norm_stream, 0)
+    step(5, 2)
+    step(6, 2)
+    for i in range(3, 7):
+        far(i)
+
+    hidden = active.shape[1]
+    ffn_in = (wg_ref, wg_in.at[0], wg_in.at[1], wg_in.at[2])
+
+    def ffn_rows(i, carry):
+        rows = pl.ds(pl.multiple_of(i * half, half), half)
+        plain = dot(xn[0, rows, :], ffn_in[0][...])
+        for s in range(1, 4):
+            plain += dot(xn[s, rows, :], ffn_in[s][...])
+        plain = plain * ffn_scale_ref[...]
+        active[rows, :] = (jax.nn.silu(plain[:, :hidden]) * plain[:, hidden:]).astype(BF16)
+        return carry
+
+    lax.fori_loop(0, tokens // half, ffn_rows, 0)
+    step(7, 2)
+    step(8, 2)
+
+    ffn_give = remote(ffn_parts.at[give], ffn_core_in, send_a.at[8], recv_a.at[8], to_core)
+    ffn_pair = [
+        remote(ffn_pair_out.at[j], ffn_pair_in.at[j], send_a.at[9 + j], recv_a.at[9 + j], to_pair)
+        for j in range(2)
+    ]
+
+    def merge_ffn():
+        ffn_give.wait_recv()
+        rows = pl.ds(steps, steps)
+        for j in range(2):
+            ffn_pair_out[j] = (
+                ffn_parts[base + j, rows, :].astype(F32) + ffn_core_in[j, rows, :].astype(F32)
+            ).astype(BF16)
+            ffn_pair[j].start()
+
+    for t in range(2):
+        if t == 1:
+            far(7)
+            far(8)
+        for s in (2 * t, 2 * t + 1):
+            project(active, ffn_out[s], 1, s, ffn_parts)
+
+        @pl.when(keep != t)
+        def _():
+            ffn_give.start()
+
+        @pl.when(keep == t)
+        def _():
+            merge_ffn()
+
+    own_rows = pl.ds(0, steps)
+    for j in range(2):
+        ffn_pair[j].wait_recv()
+        column = fx + j - 2 * fx * j
+        lanes = pl.ds(pl.multiple_of(column * width, width), width)
+        out_ref[:, lanes] = (
+            stream[base + j, own_rows, :].astype(F32)
+            + (
+                ffn_parts[base + j, own_rows, :].astype(F32)
+                + ffn_core_in[j, own_rows, :].astype(F32)
+                + ffn_pair_in[j].astype(F32)
+            )
+        ).astype(BF16)
+
+    for i in range(len(pieces)):
+        for copy in own(i) + onward(i):
+            copy.wait_send()
+    for copy in scale_copies + [x_copy, core_sums, pair_sums, mix_give, ffn_give]:
+        copy.wait_send()
+    for copy in mix_pair + stream_give + ffn_pair:
+        copy.wait_send()
+
+
+def in_one_kernel(
+
+    skip_stream_entry,
+    sequence_blender_factor,
+    product_projector,
+    product_side_factors,
+    placewise_projector,
+    placewise_entry_factors,
+    placewise_rescale_factor,
+    place_cluster_operator,
+    placewise_offset_vector,
+    blender_result_projector,
+    blender_result_factors,
+    feedforward_norm_factor,
+    switch_projector,
+    switch_factors,
+    expand_projector,
+    expand_factors,
+    contract_projector,
+    contract_factors,
+):
+    rep_index = lax.axis_index("rep")
+    tp_index = lax.axis_index("tp")
+    pair_index = rep_index % 2
+    steps, embed = skip_stream_entry.shape
+    tokens = 2 * steps
+    width = product_projector.shape[0]
+    channels = product_projector.shape[1] // 2
+    hidden = switch_projector.shape[1] // 2
+    groups = channels // GROUP_DIM
+
+    def part(values, size, dim):
+        return lax.dynamic_slice_in_dim(values, pair_index * size, size, dim)
+
+    def beside(first, second, size):
+        return jnp.concatenate(
+            (part(first, size, 1).astype(BF16), part(second, size, 1).astype(BF16)), axis=1
+        )
+
+    def scales(first, second, size):
+        return jnp.concatenate((part(first, size, 0), part(second, size, 0)))[None]
+
+    first_group = (tp_index * 2 + pair_index) * groups
+    causal = jnp.tril(jnp.ones((BLOCK, BLOCK), dtype=bool))
+    place = lax.dynamic_slice_in_dim(place_cluster_operator, first_group, groups, 0)
+    place = jnp.where(causal[None], place, jnp.zeros_like(place))
+    bias = lax.dynamic_slice_in_dim(placewise_offset_vector, first_group, groups, 0)
+    bias = jnp.repeat(bias.T, GROUP_DIM, axis=1)
+    out_scales = jnp.stack((blender_result_factors, contract_factors))
+    out_scales = jnp.concatenate((out_scales, jnp.zeros((6, width), F32)))
+
+    vmem = pltpu.VMEM
+    dma = pltpu.SemaphoreType.DMA
+    blocks = (4, tokens, width)
+    two = (2, tokens, width)
+    return pl.pallas_call(
+        functools.partial(
+            layer_kernel,
+            mixer_channels=channels,
+            all_channels=2 * channels * lax.axis_size("tp"),
+        ),
+        out_shape=jax.ShapeDtypeStruct((steps, embed // 2), BF16),
+        in_specs=[pl.BlockSpec(memory_space=vmem)] * 13,
+        out_specs=pl.BlockSpec(memory_space=vmem),
+        scratch_shapes=[
+            vmem((3, width, 2 * channels), BF16),
+            vmem((3, channels, width), BF16),
+            vmem((3, width, 2 * hidden), BF16),
+            vmem((3, hidden, width), BF16),
+            vmem((3, 8, width), F32),
+            vmem((steps, embed), BF16),
+            vmem(blocks, BF16),
+            vmem((tokens, channels), F32),
+            vmem((tokens, channels), F32),
+            vmem((tokens, channels), BF16),
+            vmem((3, 8, tokens), F32),
+            vmem((2, 8, tokens), F32),
+            vmem(blocks, BF16),
+            vmem(two, BF16),
+            vmem(two, BF16),
+            vmem(two, BF16),
+            vmem(blocks, BF16),
+            vmem((tokens, hidden), BF16),
+            vmem(blocks, BF16),
+            vmem(two, BF16),
+            vmem((2, steps, width), BF16),
+            vmem((2, steps, width), BF16),
+            dma((9, 4)),
+            dma((9, 4)),
+            dma((3,)),
+            dma((3,)),
+            dma((11,)),
+            dma((11,)),
+        ],
+        compiler_params=pltpu.CompilerParams(
+            collective_id=0, has_side_effects=True, vmem_limit_bytes=60 * 1024 * 1024
+        ),
+    )(
+        skip_stream_entry,
+        beside(product_projector, placewise_projector, channels),
+        part(blender_result_projector, channels, 0).astype(BF16),
+        beside(switch_projector, expand_projector, hidden),
+        part(contract_projector, hidden, 0).astype(BF16),
+        out_scales,
+        sequence_blender_factor[None],
+        feedforward_norm_factor[None],
+        scales(product_side_factors, placewise_entry_factors, channels),
+        part(placewise_rescale_factor, channels, 0)[None],
+        scales(switch_factors, expand_factors, hidden),
+        place,
+        bias,
+    )
+
+
+def on_device(*arrays):
+    entry, mixer, switch = arrays[0], arrays[2], arrays[12]
+    fits = (
+        lax.axis_size("rep") % 2 == 0
+        and lax.axis_size("fs") == 4
+        and lax.axis_size("tp") == 2
+        and entry.shape[0] % 256 == 0
+        and mixer.shape[0] % 128 == 0
+        and mixer.shape[1] % (2 * GROUP_DIM) == 0
+        and switch.shape[1] % 128 == 0
+    )
+    return in_one_kernel(*arrays) if fits else with_collectives(*arrays)
+
+
 def solution(mesh):
     return jax.shard_map(
         on_device,

time: 355 us -> 133 us (0.37); the launches traced: 351 us -> 133 us
  waiting for transfers between devices: 253 us -> 0 us
  Pallas kernels: 0 us -> 116 us
  matrix products: 21.2 us -> 0 us
  blocking collectives: 20.2 us -> 0 us
  local copies, waits for them, and re-layouts: 26.6 us -> 11.9 us
  between operations: 13.6 us -> 0.08 us
  other arithmetic: 16.5 us -> 5.2 us
    all_gather x4 -> x0, waiting for transfers between devices: 157 us -> none  [the longest x2 69.8 us: gathered(): lax.all_gather(jnp.concatenate((part(first, size, 1).astype(jnp.bfloat16)...]
    pallas_call x0 -> x1, Pallas kernels: none -> 116 us  [in_one_kernel(): pl.pallas_call(functools.partial(layer_kernel, mixer_channels=channels, a...]
    reduce_scatter x2 -> x0, waiting for transfers between devices: 95.6 us -> none  [the longest x1 48.3 us: on_device(): lax.psum_scatter(ffn_terms.reshape(rep * tp * steps, own_features), group...]
    dot_general x5 -> x0, matrix products: 21.2 us -> none  [the longest x2 10.2 us: projected(): lax.dot_general(values, weights, (((1,), (1,)), ((), ())), preferred_elem...]
    reshape x2 -> x0, local copies, waits for them, and re-layouts: 13.3 us -> none  [on_device(): ffn_terms.reshape(rep, steps, tp, own_features).transpose(0, 2, 1, 3)]
    psum x1 -> x0, blocking collectives: 13.2 us -> none  [on_device(): squares = lax.psum(jnp.sum(spread * spread, axis=1), group)]
    convert_element_type x5 -> x0, other arithmetic: 8.87 us -> none  [the longest x1 2.19 us: on_device(): (own_stream.astype(jnp.float32) + ffn_total.astype(jnp.float32)).astype(j...]
    all_gather x1 -> x0, blocking collectives: 6.99 us -> none  [on_device(): lax.all_gather(jnp.stack((blender_result_factors, contract_factors)), 'fs...]
  transfers between devices with their start and end apart: 6 -> 0, of which waited for: 6 -> 0; matrix products, arithmetic and copies ran while one was open for 5% -> 0% of each run, Pallas kernels for 0% -> 0%
where the time goes in v2:
time: 133 us
  Pallas kernels  116 us (87%)
  local copies, waits for them, and re-layouts  11.9 us (9%)
  other arithmetic  5.2 us (4%)
    pallas_call x1, Pallas kernels, in_one_kernel(): pl.pallas_call(functools.partial(layer_kernel, mixer_channels=channels, a...  116 us
    convert_element_type x2, local copies, waits for them, and re-layouts, beside(): part(second, size, 1).astype(BF16)  4 us

profile of v2, /device:TPU:1, one launch (start us, length us, event | category | flops | bytes accessed | tf_op | source)
XLA Modules:
  0.0 133.0 jit_solution(17542285167395647783)
XLA Ops:
  0.0 0.0 copy-start
  0.0 2.7 %dynamic-slice_convert_fusion = (bf16[512,704]{1,0:T(8,128)(2,1)S(1)}, bf16[512,704]{1,0:T(8,128)(2,1)S(1)}) fusion(f32[512,1408]{1,0:T(8,128)} %param.32, s32[]{:T(128)S(6)} %select_n.34, f32[512,1408]{1,0:T(8,128)} %param.30), kind=kLoop, calls=%fused_computation | loop fusion | bytes 2883588 | tf_op jit(solution)/shard_map/convert_element_type | solution.py:541
  2.7 1.6 %pad_maximum_fusion.wg_ref = bf16[512,1408]{1,0:T(8,128)(2,1)} fusion(bf16[512,704]{1,0:T(8,128)(2,1)S(1)} %get-tuple-element.7, bf16[512,704]{1,0:T(8,128)(2,1)S(1)} %get-tuple-element.8), kind=kLoop, calls=%fused_computation.2 | loop fusion | flops 2883584 | bytes 2883584 | tf_op jit(solution)/shard_map/concatenate | solution.py:540
  4.3 0.0 copy-start.7
  4.3 0.0 copy-start.3
  4.3 0.0 copy-start.4
  4.3 1.3 dynamic-slice_convert_fusion.4
  5.6 0.8 pad_maximum_fusion.1.wm_ref
  6.5 0.0 copy-done
  6.5 1.0 dynamic-slice_convert_fusion.2.wc_ref
  7.4 0.7 fusion
  8.1 0.1 copy.19
  8.2 0.2 broadcast_in_dim.44
  8.4 0.7 copy.22
  9.1 1.8 %dynamic-slice_convert_fusion.3.wb_ref = bf16[256,512]{1,0:T(8,128)(2,1)} fusion(f32[512,512]{1,0:T(8,128)} %param.27, s32[]{:T(128)S(6)} %select_n.20), kind=kLoop, calls=%fused_computation.5 | loop fusion | bytes 524292 | tf_op jit(solution)/shard_map/convert_element_type | solution.py:605
  10.9 1.5 %dynamic-slice_select_fusion.place_ref = bf16[2,128,128]{2,1,0:T(8,128)(2,1)} fusion(bf16[8,128,128]{2,1,0:T(8,128)(2,1)} %param.25, s32[]{:T(128)S(6)} %select_n.35, pred[128,128]{1,0:T(8,128)(4,1)S(1)} %iota_compare_fusion), kind=kLoop, calls=%fused_computation.9 | loop fusion | flops 32768 | bytes 147460 | tf_op jit(solution)/shard_map/jit(_where)/select_n | solution.py:550
  12.3 0.0 copy-done.1
  12.4 0.1 dynamic_slice.48
  12.4 0.0 copy-done.2
  12.4 0.1 dynamic_slice.49
  12.5 0.1 pad_maximum_fusion.2
  12.6 0.6 broadcast_in_dim.41.ffn_scale_ref
  13.2 0.0 copy-done.5
  13.2 0.1 dynamic_slice.45
  13.3 0.0 copy-done.6
  13.3 0.1 dynamic_slice.46
  13.3 0.6 pad_maximum_fusion.3
  13.9 0.6 dynamic_slice.47
  14.5 0.1 pad.6.clone
  14.6 0.7 maximum_maximum_fusion.sc_ref
  15.3 115.9 %shard_map.172 = bf16[256,1024]{1,0:T(8,128)(2,1)} custom-call(bf16[256,2048]{1,0:T(8,128)(2,1)} %x_ref.1, bf16[512,512]{1,0:T(8,128)(2,1)} %pad_maximum_fusion.1.wm_ref, bf16[256,512]{1,0:T(8,128)(2,1)} %dynamic-slice_convert_fusion.3.wb_ref, bf16[512,1408]{1,0:T(8,128)(2,1)} %pad_maximum_fusion.wg_ref, ...), custom_call_target="tpu_custom_call" | custom-call | tf_op jit(solution)/shard_map/pallas_call | solution.py:560
  131.2 1.9 %copy.24 = bf16[256,1024]{1,0:T(8,128)(2,1)} copy(bf16[256,1024]{1,0:T(8,128)(2,1)} %shard_map.172) | data formatting | bytes 1048576
  (9 shorter events, 0.0 us)
Async XLA Ops:
  0.0 6.5 %copy-start = (f32[1408,512]{1,0:T(8,128)S(1)}, f32[1408,512]{1,0:T(8,128)}, u32[]{:S(2)}) copy-start(f32[1408,512]{1,0:T(8,128)} %param.34) | copy-start | bytes 8650756
  4.3 8.1 %copy-start.1 = (f32[1408]{0:T(1024)S(1)}, f32[1408]{0:T(1024)}, u32[]{:S(2)}) copy-start(f32[1408]{0:T(1024)} %param.31) | copy-start | bytes 16900
  4.3 8.2 %copy-start.2 = (f32[1408]{0:T(1024)S(1)}, f32[1408]{0:T(1024)}, u32[]{:S(2)}) copy-start(f32[1408]{0:T(1024)} %param.33) | copy-start | bytes 16900
  4.3 8.9 %copy-start.5 = (f32[512]{0:T(512)S(1)}, f32[512]{0:T(512)}, u32[]{:S(2)}) copy-start(f32[512]{0:T(512)} %param.21) | copy-start | bytes 6148
  4.3 9.0 %copy-start.6 = (f32[512]{0:T(512)S(1)}, f32[512]{0:T(512)}, u32[]{:S(2)}) copy-start(f32[512]{0:T(512)} %param.23) | copy-start | bytes 6148
  4.3 9.7 %copy-start.7 = (f32[512]{0:T(512)S(1)}, f32[512]{0:T(512)}, u32[]{:S(2)}) copy-start(f32[512]{0:T(512)} %param.24) | copy-start | bytes 6148
  4.3 10.3 %copy-start.3 = (f32[512]{0:T(512)S(1)}, f32[512]{0:T(512)}, u32[]{:S(2)}) copy-start(f32[512]{0:T(512)} %param.35) | copy-start | bytes 6148
  4.3 10.3 %copy-start.4 = (f32[512]{0:T(512)S(1)}, f32[512]{0:T(512)}, u32[]{:S(2)}) copy-start(f32[512]{0:T(512)} %param.28) | copy-start | bytes 6148

commit v3 on v2

--- a/solution.py
+++ b/solution.py
@@ -151,19 +151,33 @@
 
 def layer_kernel(
     x_ref,
+    product_ref,
+    placewise_ref,
+    blender_ref,
+    switch_ref,
+    expand_ref,
+    contract_ref,
+    gain_ref,
+    ffn_gain_ref,
+    product_scale_ref,
+    placewise_scale_ref,
+    rescale_ref,
+    switch_scale_ref,
+    expand_scale_ref,
+    mix_scale_ref,
+    contract_scale_ref,
+    place_ref,
+    bias_ref,
+    out_ref,
     wm_ref,
     wb_ref,
     wg_ref,
     wc_ref,
     sc_ref,
-    gain_ref,
-    ffn_gain_ref,
-    mixer_scale_ref,
-    rescale_ref,
-    ffn_scale_ref,
-    place_ref,
-    bias_ref,
-    out_ref,
+    wm_wide,
+    wb_wide,
+    wg_wide,
+    wc_wide,
     wm_in,
     wb_in,
     wg_in,
@@ -192,6 +206,7 @@
     recv_sc,
     send_a,
     recv_a,
+    load,
     mixer_channels,
     all_channels,
 ):
@@ -206,6 +221,31 @@
     steps = x_ref.shape[0]
     tokens = 2 * steps
     width = wm_ref.shape[0]
+    h = r % 2
+    hidden = active.shape[1]
+    shard = pl.ds(pl.multiple_of(h * mixer_channels, mixer_channels), mixer_channels)
+    units = pl.ds(pl.multiple_of(h * hidden, 8), hidden)
+    loads = [
+        pltpu.make_async_copy(src, dst, load.at[i])
+        for i, (src, dst) in enumerate(
+            (
+                (product_ref.at[:, shard], wm_wide.at[0]),
+                (placewise_ref.at[:, shard], wm_wide.at[1]),
+                (blender_ref.at[shard], wb_wide),
+                (switch_ref, wg_wide.at[0]),
+                (expand_ref, wg_wide.at[1]),
+                (contract_ref.at[units], wc_wide),
+            )
+        )
+    ]
+    for copy in loads:
+        copy.start()
+
+    def chosen(values):
+        return jnp.where(h == 0, values[:, :hidden], values[:, hidden:])
+
+    first_row = lax.broadcasted_iota(jnp.int32, sc_ref.shape, 0) == 0
+    sc_ref[...] = jnp.where(first_row, mix_scale_ref[...], contract_scale_ref[...])
 
     barrier = pltpu.get_barrier_semaphore()
     for other in (to_x, to_y, to_d, to_pair, to_core):
@@ -261,11 +301,30 @@
         for s, device in enumerate((to_x, to_y, to_d))
     ]
     x_copy = remote(x_ref, x_in, send_a.at[0], recv_a.at[0], to_pair)
+    loads[0].wait()
+    loads[1].wait()
+    wm_ref[:, :mixer_channels] = wm_wide[0].astype(BF16)
+    wm_ref[:, mixer_channels:] = wm_wide[1].astype(BF16)
+    x_copy.start()
     for copy in scale_copies:
         copy.start()
     issue(0)
-    x_copy.start()
     issue(1)
+    loads[2].wait()
+    wb_ref[...] = wb_wide[...].astype(BF16)
+    loads[3].wait()
+    loads[4].wait()
+
+    def round_ffn(i, carry):
+        rows = pl.ds(pl.multiple_of(i * 64, 64), 64)
+        wg_ref[rows, :] = jnp.concatenate(
+            (chosen(wg_wide[0, rows, :]), chosen(wg_wide[1, rows, :])), axis=1
+        ).astype(BF16)
+        return carry
+
+    lax.fori_loop(0, width // 64, round_ffn, 0)
+    loads[5].wait()
+    wc_ref[...] = wc_wide[...].astype(BF16)
 
     def feature(s):
         return pl.ds(pl.multiple_of(seat[s] * width, width), width)
@@ -307,7 +366,10 @@
         plain = dot(xn[0, rows, :], mixer_in[0][...])
         for s in range(1, 4):
             plain += dot(xn[s, rows, :], mixer_in[s][...])
-        both = jax.nn.gelu(plain * mixer_scale_ref[...])
+        column_scales = jnp.concatenate(
+            (product_scale_ref[:, shard], placewise_scale_ref[:, shard]), axis=1
+        )
+        both = jax.nn.gelu(plain * column_scales)
         carrier[rows, :] = both[:, :mixer_channels]
         own_spread = both[:, mixer_channels:]
         spread[rows, :] = own_spread
@@ -323,19 +385,29 @@
     pair_sums = remote(sums.at[1], sums_in.at[1], send_a.at[2], recv_a.at[2], to_pair)
     pair_sums.start()
     step(2, 2)
+    issue(5)
     pair_sums.wait_recv()
     received = sums_in[1]
     received = jnp.concatenate((received[:, steps:], received[:, :steps]), axis=1)
     sums[2] = lax.rsqrt((sums[1] + received) / all_channels + epsilon)
 
+    causal = lax.broadcasted_iota(jnp.int32, (BLOCK, BLOCK), 0) >= lax.broadcasted_iota(
+        jnp.int32, (BLOCK, BLOCK), 1
+    )
+    groups = mixer_channels // GROUP_DIM
+    first_group = (2 * k + h) * groups
+
     def mix_rows(i, carry):
         rows = pl.ds(pl.multiple_of(i * BLOCK, BLOCK), BLOCK)
         factor = jnp.concatenate([sums[2, :, rows]] * (128 // 8), axis=0).T[:, :1]
-        normed = (spread[rows, :] * factor * rescale_ref[...]).astype(BF16)
-        for g in range(mixer_channels // GROUP_DIM):
+        normed = (spread[rows, :] * factor * rescale_ref[:, shard]).astype(BF16)
+        for g in range(groups):
             lanes = pl.ds(g * GROUP_DIM, GROUP_DIM)
-            mixed = dot(place_ref[g], normed[:, g * GROUP_DIM : (g + 1) * GROUP_DIM])
-            mixed = mixed + bias_ref[:, lanes]
+            operator = place_ref[first_group + g]
+            operator = jnp.where(causal, operator, jnp.zeros_like(operator))
+            offset = jnp.broadcast_to(bias_ref[pl.ds(first_group + g, 1), :], (BLOCK, BLOCK)).T
+            mixed = dot(operator, normed[:, g * GROUP_DIM : (g + 1) * GROUP_DIM])
+            mixed = mixed + offset
             gated[rows, lanes] = (carrier[rows, lanes] * mixed).astype(BF16)
         return carry
 
@@ -393,8 +465,8 @@
         def _():
             merge_mix()
 
-    step(3, 2)
-    step(4, 2)
+    step(3, 3)
+    step(4, len(pieces))
 
     stream_give = [
         remote(stream.at[base + j], stream.at[base + j], send_a.at[6 + j], recv_a.at[6 + j], to_core)
@@ -433,7 +505,6 @@
     for i in range(3, 7):
         far(i)
 
-    hidden = active.shape[1]
     ffn_in = (wg_ref, wg_in.at[0], wg_in.at[1], wg_in.at[2])
 
     def ffn_rows(i, carry):
@@ -441,7 +512,9 @@
         plain = dot(xn[0, rows, :], ffn_in[0][...])
         for s in range(1, 4):
             plain += dot(xn[s, rows, :], ffn_in[s][...])
-        plain = plain * ffn_scale_ref[...]
+        plain = plain * jnp.concatenate(
+            (chosen(switch_scale_ref[...]), chosen(expand_scale_ref[...])), axis=1
+        )
         active[rows, :] = (jax.nn.silu(plain[:, :hidden]) * plain[:, hidden:]).astype(BF16)
         return carry
 
@@ -523,35 +596,11 @@
     contract_projector,
     contract_factors,
 ):
-    rep_index = lax.axis_index("rep")
-    tp_index = lax.axis_index("tp")
-    pair_index = rep_index % 2
     steps, embed = skip_stream_entry.shape
     tokens = 2 * steps
     width = product_projector.shape[0]
     channels = product_projector.shape[1] // 2
     hidden = switch_projector.shape[1] // 2
-    groups = channels // GROUP_DIM
-
-    def part(values, size, dim):
-        return lax.dynamic_slice_in_dim(values, pair_index * size, size, dim)
-
-    def beside(first, second, size):
-        return jnp.concatenate(
-            (part(first, size, 1).astype(BF16), part(second, size, 1).astype(BF16)), axis=1
-        )
-
-    def scales(first, second, size):
-        return jnp.concatenate((part(first, size, 0), part(second, size, 0)))[None]
-
-    first_group = (tp_index * 2 + pair_index) * groups
-    causal = jnp.tril(jnp.ones((BLOCK, BLOCK), dtype=bool))
-    place = lax.dynamic_slice_in_dim(place_cluster_operator, first_group, groups, 0)
-    place = jnp.where(causal[None], place, jnp.zeros_like(place))
-    bias = lax.dynamic_slice_in_dim(placewise_offset_vector, first_group, groups, 0)
-    bias = jnp.repeat(bias.T, GROUP_DIM, axis=1)
-    out_scales = jnp.stack((blender_result_factors, contract_factors))
-    out_scales = jnp.concatenate((out_scales, jnp.zeros((6, width), F32)))
 
     vmem = pltpu.VMEM
     dma = pltpu.SemaphoreType.DMA
@@ -564,9 +613,20 @@
             all_channels=2 * channels * lax.axis_size("tp"),
         ),
         out_shape=jax.ShapeDtypeStruct((steps, embed // 2), BF16),
-        in_specs=[pl.BlockSpec(memory_space=vmem)] * 13,
+        in_specs=[pl.BlockSpec(memory_space=vmem)]
+        + [pl.BlockSpec(memory_space=pl.ANY)] * 6
+        + [pl.BlockSpec(memory_space=vmem)] * 11,
         out_specs=pl.BlockSpec(memory_space=vmem),
         scratch_shapes=[
+            vmem((width, 2 * channels), BF16),
+            vmem((channels, width), BF16),
+            vmem((width, 2 * hidden), BF16),
+            vmem((hidden, width), BF16),
+            vmem((8, width), F32),
+            vmem((2, width, channels), F32),
+            vmem((channels, width), F32),
+            vmem((2, width, 2 * hidden), F32),
+            vmem((hidden, width), F32),
             vmem((3, width, 2 * channels), BF16),
             vmem((3, channels, width), BF16),
             vmem((3, width, 2 * hidden), BF16),
@@ -595,24 +655,30 @@
             dma((3,)),
             dma((11,)),
             dma((11,)),
+            dma((6,)),
         ],
         compiler_params=pltpu.CompilerParams(
             collective_id=0, has_side_effects=True, vmem_limit_bytes=60 * 1024 * 1024
         ),
     )(
         skip_stream_entry,
-        beside(product_projector, placewise_projector, channels),
-        part(blender_result_projector, channels, 0).astype(BF16),
-        beside(switch_projector, expand_projector, hidden),
-        part(contract_projector, hidden, 0).astype(BF16),
-        out_scales,
+        product_projector,
+        placewise_projector,
+        blender_result_projector,
+        switch_projector,
+        expand_projector,
+        contract_projector,
         sequence_blender_factor[None],
         feedforward_norm_factor[None],
-        scales(product_side_factors, placewise_entry_factors, channels),
-        part(placewise_rescale_factor, channels, 0)[None],
-        scales(switch_factors, expand_factors, hidden),
-        place,
-        bias,
+        product_side_factors[None],
+        placewise_entry_factors[None],
+        placewise_rescale_factor[None],
+        switch_factors[None],
+        expand_factors[None],
+        blender_result_factors[None],
+        contract_factors[None],
+        place_cluster_operator,
+        placewise_offset_vector,
     )
 
 

time: 133 us -> 120 us (0.902)
  local copies, waits for them, and re-layouts: 11.9 us -> 4.45 us
  other arithmetic: 5.2 us -> 0 us
    convert_element_type x4 -> x0, local copies, waits for them, and re-layouts: 6.74 us -> none  [the longest x2 4 us: beside(): part(second, size, 1).astype(BF16)]
    concatenate x5 -> x0, other arithmetic: 3.72 us -> none  [the longest x2 2.39 us: beside(): jnp.concatenate((part(first, size, 1).astype(BF16), part(second, size, 1)...]
    broadcast_in_dim x3 -> x2, local copies, waits for them, and re-layouts: 0.8 us -> 2.59 us  [the longest x1 1.29 us: in_one_kernel(): switch_factors[None]]
    select_n x1 -> x0, other arithmetic: 1.47 us -> none  [in_one_kernel(): place = jnp.where(causal[None], place, jnp.zeros_like(place))]
where the time goes in v3:
time: 120 us
  Pallas kernels  115 us (96%)
  local copies, waits for them, and re-layouts  4.45 us (4%)
    pallas_call x1, Pallas kernels, in_one_kernel(): pl.pallas_call(functools.partial(layer_kernel, mixer_channels=channels, a...  115 us

profile of v3, /device:TPU:1, one launch (start us, length us, event | category | flops | bytes accessed | tf_op | source)
XLA Modules:
  0.0 119.8 jit_solution(11436730394280807368)
XLA Ops:
  0.0 1.3 %broadcast_in_dim.32.switch_scale_ref = f32[1,1408]{1,0:T(1,128)} reshape(f32[1408]{0:T(1024)} %param.31) | data formatting | bytes 11264 | tf_op jit(solution)/shard_map/broadcast_in_dim | solution.py:676
  1.3 1.3 %broadcast_in_dim.33.expand_scale_ref = f32[1,1408]{1,0:T(1,128)} reshape(f32[1408]{0:T(1024)} %param.33) | data formatting | bytes 11264 | tf_op jit(solution)/shard_map/broadcast_in_dim | solution.py:677
  2.6 115.4 %shard_map.172 = bf16[256,1024]{1,0:T(8,128)(2,1)} custom-call(bf16[256,2048]{1,0:T(8,128)(2,1)} %x_ref.1, f32[512,512]{1,0:T(8,128)} %product_ref.1, f32[512,512]{1,0:T(8,128)} %placewise_ref.1, f32[512,512]{1,0:T(8,128)} %blender_ref.1, f32[512,1408]{1,0:T(8,128)} %switch_ref.1, f32[512,1408]{1,0:T(8,128)} %expand_ref.1, f32[1408,512]{1,0:T(8,128)} %contract_ref.1, ...), custom_call_target="tpu_custom_call" | custom-call | tf_op jit(solution)/shard_map/pallas_call | solution.py:609
  118.0 1.9 %copy.20 = bf16[256,1024]{1,0:T(8,128)(2,1)} copy(bf16[256,1024]{1,0:T(8,128)(2,1)} %shard_map.172) | data formatting | bytes 1048576

commit v4 on v3

--- a/solution.py
+++ b/solution.py
@@ -513,7 +513,10 @@
         for s in range(1, 4):
             plain += dot(xn[s, rows, :], ffn_in[s][...])
         plain = plain * jnp.concatenate(
-            (chosen(switch_scale_ref[...]), chosen(expand_scale_ref[...])), axis=1
+            (
+                chosen(switch_scale_ref[...][None]),
+                chosen(expand_scale_ref[...][None]),
+            ), axis=1
         )
         active[rows, :] = (jax.nn.silu(plain[:, :hidden]) * plain[:, hidden:]).astype(BF16)
         return carry
@@ -522,35 +525,37 @@
     step(7, 2)
     step(8, 2)
 
-    ffn_give = remote(ffn_parts.at[give], ffn_core_in, send_a.at[8], recv_a.at[8], to_core)
+    ffn_give = [
+        remote(ffn_parts.at[2 - base + j], ffn_core_in.at[j], send_a.at[i], recv_a.at[i], to_core)
+        for j, i in enumerate((8, 11))
+    ]
     ffn_pair = [
         remote(ffn_pair_out.at[j], ffn_pair_in.at[j], send_a.at[9 + j], recv_a.at[9 + j], to_pair)
         for j in range(2)
     ]
 
-    def merge_ffn():
-        ffn_give.wait_recv()
+    def merge_ffn(j):
+        ffn_give[j].wait_recv()
         rows = pl.ds(steps, steps)
-        for j in range(2):
-            ffn_pair_out[j] = (
-                ffn_parts[base + j, rows, :].astype(F32) + ffn_core_in[j, rows, :].astype(F32)
-            ).astype(BF16)
-            ffn_pair[j].start()
-
-    for t in range(2):
-        if t == 1:
+        ffn_pair_out[j] = (
+            ffn_parts[base + j, rows, :].astype(F32) + ffn_core_in[j, rows, :].astype(F32)
+        ).astype(BF16)
+        ffn_pair[j].start()
+
+    for s in range(4):
+        t, j = s // 2, s % 2
+        if s == 3:
             far(7)
             far(8)
-        for s in (2 * t, 2 * t + 1):
-            project(active, ffn_out[s], 1, s, ffn_parts)
+        project(active, ffn_out[s], 1, s, ffn_parts)
 
         @pl.when(keep != t)
         def _():
-            ffn_give.start()
+            ffn_give[j].start()
 
         @pl.when(keep == t)
         def _():
-            merge_ffn()
+            merge_ffn(j)
 
     own_rows = pl.ds(0, steps)
     for j in range(2):
@@ -569,7 +574,7 @@
     for i in range(len(pieces)):
         for copy in own(i) + onward(i):
             copy.wait_send()
-    for copy in scale_copies + [x_copy, core_sums, pair_sums, mix_give, ffn_give]:
+    for copy in scale_copies + [x_copy, core_sums, pair_sums, mix_give] + ffn_give:
         copy.wait_send()
     for copy in mix_pair + stream_give + ffn_pair:
         copy.wait_send()
@@ -653,8 +658,8 @@
             dma((9, 4)),
             dma((3,)),
             dma((3,)),
-            dma((11,)),
-            dma((11,)),
+            dma((12,)),
+            dma((12,)),
             dma((6,)),
         ],
         compiler_params=pltpu.CompilerParams(
@@ -673,8 +678,8 @@
         product_side_factors[None],
         placewise_entry_factors[None],
         placewise_rescale_factor[None],
-        switch_factors[None],
-        expand_factors[None],
+        switch_factors,
+        expand_factors,
         blender_result_factors[None],
         contract_factors[None],
         place_cluster_operator,

time: 120 us -> 114 us (0.950)
  Pallas kernels: 115 us -> 112 us
  local copies, waits for them, and re-layouts: 4.45 us -> 1.87 us
    pallas_call x1, Pallas kernels: 115 us -> 112 us  [in_one_kernel(): pl.pallas_call(functools.partial(layer_kernel, mixer_channels=channels, a...]
    broadcast_in_dim x2 -> x0, local copies, waits for them, and re-layouts: 2.59 us -> none  [the longest x1 1.29 us: in_one_kernel(): switch_factors[None]]
where the time goes in v4:
time: 114 us
  Pallas kernels  112 us (98%)
  local copies, waits for them, and re-layouts  1.87 us (2%)
    pallas_call x1, Pallas kernels, in_one_kernel(): pl.pallas_call(functools.partial(layer_kernel, mixer_channels=channels, a...  112 us

profile of v4, /device:TPU:1, one launch (start us, length us, event | category | flops | bytes accessed | tf_op | source)
XLA Modules:
  0.0 113.6 jit_solution(1695006034587546709)
XLA Ops:
  0.0 111.7 %shard_map.172 = bf16[256,1024]{1,0:T(8,128)(2,1)} custom-call(bf16[256,2048]{1,0:T(8,128)(2,1)} %x_ref.1, f32[512,512]{1,0:T(8,128)} %product_ref.1, f32[512,512]{1,0:T(8,128)} %placewise_ref.1, f32[512,512]{1,0:T(8,128)} %blender_ref.1, f32[512,1408]{1,0:T(8,128)} %switch_ref.1, f32[512,1408]{1,0:T(8,128)} %expand_ref.1, f32[1408,512]{1,0:T(8,128)} %contract_ref.1, ...), custom_call_target="tpu_custom_call" | custom-call | tf_op jit(solution)/shard_map/pallas_call | solution.py:614
  111.7 1.9 %copy.20 = bf16[256,1024]{1,0:T(8,128)(2,1)} copy(bf16[256,1024]{1,0:T(8,128)(2,1)} %shard_map.172) | data formatting | bytes 1048576
